TPU v7x, 32 devices: a whole 2x2x4 slice. The times are simulated.
32 devices in a mesh: ep: 8 (over z, y), tp: 4 (over x, core).
Axes of the slice: x: 2, y: 2, z: 4, core: 2. Of those that a mesh axis runs over, the one named last changes fastest.
Arguments:
- q_latent: bfloat16 [4096, 512], P(('ep', 'tp')), may hold values from -6 to 6
- kv_latent: bfloat16 [4096, 256], P(('ep', 'tp')), may hold values from -6 to 6
- rope_key: bfloat16 [4096, 32], P(('ep', 'tp')), may hold values from -240 to 240
- q_gain: float32 [512], replicated, may hold values from 0.1 to 1.9
- kv_gain: float32 [256], replicated, may hold values from 0.1 to 1.9
- w_query: bfloat16 [512, 1024], P(None, 'tp'), may hold values from -0.25 to 0.25
- w_query_rot: bfloat16 [512, 512], P(None, 'tp'), may hold values from -0.25 to 0.25
- w_key: bfloat16 [256, 1024], P(None, 'tp'), may hold values from -0.375 to 0.375
- w_value: bfloat16 [256, 1024], P(None, 'tp'), may hold values from -0.375 to 0.375
- w_mix_out: bfloat16 [1024, 2048], P('tp'), may hold values from -0.1875 to 0.1875
- expert_input: bfloat16 [4096, 2048], P(('ep', 'tp')), may hold values from -6 to 6
- ffn_gain: float32 [2048], replicated, may hold values from 0.1 to 1.9
- expert_ids: int32 [4096, 4], P(('ep', 'tp')), may hold values from 0 to 7, all different within a row; in each aligned block of 128 rows (0 to 127, 128 to 255, ...) at most 96 rows name the same one
- route_weights: float32 [4096, 4], P(('ep', 'tp')), may hold values from 0.2 to 1
- w_gate_exp: bfloat16 [8, 2048, 1024], P('ep', None, 'tp'), may hold values from -0.125 to 0.125
- w_up_exp: bfloat16 [8, 2048, 1024], P('ep', None, 'tp'), may hold values from -0.125 to 0.125
- w_down_exp: bfloat16 [8, 1024, 2048], P('ep', 'tp'), may hold values from -0.1875 to 0.1875
Outputs:
- mixer_out: bfloat16 [4096, 2048], P(('ep', 'tp'))
- expert_out: bfloat16 [4096, 2048], P(('ep', 'tp'))
Inputs may be any that keep to these rules, and one draw needn't show every extreme that they name: `expert_ids`: the experts of a row are all different. In the rows of one device (aligned blocks of 128 tokens) no expert is named by more than 96 rows, a bound that some block reaches.
All inputs are finite; a program needn't handle non-finite values.
Results may differ from a plain program's by a relative error of at most 0.012.
The roundings to bfloat16 on the way count: a program that leaves them out, or rounds other values in their place, can miss the bound.
Values may be sent and summed in bfloat16 or wider, within the bound.
A program may use at most 128 MiB of HBM per device.

v0:
```python
import functools
import math

import jax
import jax.numpy as jnp
from jax import lax
from jax.experimental import pallas as pl
from jax.experimental.pallas import tpu as pltpu
from jax.sharding import PartitionSpec as P

D = 2048
NOPE = 64
ROPE = 32
VD = 64
TOPK = 4
SEG = 64


norm_epsilon = 1e-06
rope_base = 10000.0
masked_score = -1e30


def rms_scale(values_in, gain_vec):
    floats = values_in.astype(jnp.float32)
    return (
        floats
        * lax.rsqrt(jnp.mean(floats * floats, axis=-1, keepdims=True) + norm_epsilon)
        * gain_vec
    )


def tables(positions):
    half_width = ROPE // 2
    frequency = rope_base ** (-jnp.arange(half_width, dtype=jnp.float32) / half_width)
    angles = positions.astype(jnp.float32)[:, None] * frequency[None, :]
    return (jnp.cos(angles), jnp.sin(angles))


def rotate_pairs(values_in, cosine, sine_table):
    half_width = values_in.shape[-1] // 2
    first, second = (values_in[..., :half_width], values_in[..., half_width:])
    return jnp.concatenate(
        [first * cosine - second * sine_table, first * sine_table + second * cosine], axis=-1
    )


LANES = 128


def pad_heads(weight, heads, width):
    split = weight.reshape(weight.shape[0], heads, width)
    return jnp.pad(split, ((0, 0), (0, 0), (0, LANES - width))).reshape(
        weight.shape[0], heads * LANES
    )


def make_queries(q_rows, q_gain, w_query, w_query_rot, heads, group_rows):
    start = lax.axis_index("ep") * group_rows
    cosine, sine_table = tables(start + jnp.arange(group_rows, dtype=jnp.int32))
    normed = rms_scale(q_rows, q_gain).astype(jnp.bfloat16)
    plain = jnp.dot(normed, w_query, preferred_element_type=jnp.float32).astype(jnp.bfloat16)
    turned = jnp.dot(normed, w_query_rot, preferred_element_type=jnp.float32).reshape(
        group_rows, heads, ROPE
    )
    turned = rotate_pairs(turned, cosine[:, None, :], sine_table[:, None, :]).astype(jnp.bfloat16)
    blank = jnp.zeros((group_rows, heads, LANES - NOPE - ROPE), jnp.bfloat16)
    joined = jnp.concatenate([plain.reshape(group_rows, heads, NOPE), turned, blank], axis=-1)
    return joined.reshape(group_rows, heads * LANES)


def make_keys(kv_rows, kv_gain, w_key, w_value, heads):
    row_count = kv_rows.shape[0]
    rank = w_key.shape[0]
    normed = rms_scale(kv_rows[:, :rank], kv_gain).astype(jnp.bfloat16)
    cosine, sine_table = tables(jnp.arange(row_count, dtype=jnp.int32))
    turned = rotate_pairs(kv_rows[:, rank:].astype(jnp.float32), cosine, sine_table)
    turned = jnp.pad(
        turned.astype(jnp.bfloat16), ((0, 0), (NOPE, LANES - NOPE - ROPE))
    )
    plain = jnp.dot(normed, pad_heads(w_key, heads, NOPE), preferred_element_type=jnp.float32)
    keys = plain.astype(jnp.bfloat16) + jnp.tile(turned, (1, heads))
    raw = jnp.dot(normed, pad_heads(w_value, heads, VD), preferred_element_type=jnp.float32)
    ones = (jnp.arange(heads * LANES, dtype=jnp.int32) % LANES == VD).astype(jnp.bfloat16)
    return keys, raw.astype(jnp.bfloat16) + ones[None, :]


def attention_kernel(heads, chunk, group_ref, q_ref, k_ref, v_ref, o_ref, max_ref, acc_ref):
    step = pl.program_id(0)
    group = group_ref[0]
    rows = q_ref.shape[0]
    keys = k_ref.shape[0]
    log_scale = (NOPE + ROPE) ** (-0.5) * math.log2(math.e)

    @pl.when(step == 0)
    def _():
        max_ref[...] = jnp.full(max_ref.shape, masked_score, jnp.float32)
        acc_ref[...] = jnp.zeros(acc_ref.shape, jnp.float32)

    def work(masked):
        for head in range(heads):
            lanes = slice(head * LANES, (head + 1) * LANES)
            for first in range(0, rows, chunk):
                part = slice(first, first + chunk)
                scores = lax.dot_general(
                    q_ref[part, lanes],
                    k_ref[:, lanes],
                    (((1,), (1,)), ((), ())),
                    preferred_element_type=jnp.float32,
                )
                if masked:
                    row_id = lax.broadcasted_iota(jnp.int32, (chunk, keys), 0) + first
                    col_id = lax.broadcasted_iota(jnp.int32, (chunk, keys), 1)
                    scores = jnp.where(col_id // SEG <= row_id // SEG, scores, masked_score)
                old = max_ref[head, part, :]
                new = jnp.maximum(old, jnp.max(scores, axis=-1, keepdims=True))
                weights = jnp.exp2((scores - new[:, :1]) * log_scale).astype(jnp.bfloat16)
                factor = jnp.exp2((old - new) * log_scale)
                max_ref[head, part, :] = new
                acc_ref[head, part, :] = acc_ref[head, part, :] * factor + jnp.dot(
                    weights, v_ref[:, lanes], preferred_element_type=jnp.float32
                )

    @pl.when(step < group)
    def _():
        work(False)

    @pl.when(step == group)
    def _():
        work(True)

    @pl.when(step == pl.num_programs(0) - 1)
    def _():
        for head in range(heads):
            acc = acc_ref[head]
            o_ref[:, head * VD : (head + 1) * VD] = (
                acc[:, :VD] / acc[:, VD : VD + 1]
            ).astype(jnp.bfloat16)


def attend(queries, keys, values, heads, group_rows):
    group = lax.axis_index("ep").astype(jnp.int32).reshape(1)
    blocks = keys.shape[0] // group_rows
    width = heads * LANES
    chunk = 256 if group_rows % 256 == 0 else group_rows
    return pl.pallas_call(
        functools.partial(attention_kernel, heads, chunk),
        out_shape=jax.ShapeDtypeStruct((group_rows, heads * VD), jnp.bfloat16),
        grid_spec=pltpu.PrefetchScalarGridSpec(
            num_scalar_prefetch=1,
            grid=(blocks,),
            in_specs=[
                pl.BlockSpec((group_rows, width), lambda i, g: (0, 0)),
                pl.BlockSpec((group_rows, width), lambda i, g: (jnp.minimum(i, g[0]), 0)),
                pl.BlockSpec((group_rows, width), lambda i, g: (jnp.minimum(i, g[0]), 0)),
            ],
            out_specs=pl.BlockSpec((group_rows, heads * VD), lambda i, g: (0, 0)),
            scratch_shapes=[
                pltpu.VMEM((heads, group_rows, LANES), jnp.float32),
                pltpu.VMEM((heads, group_rows, LANES), jnp.float32),
            ],
        ),
        compiler_params=pltpu.CompilerParams(
            dimension_semantics=("arbitrary",), vmem_limit_bytes=24 * 1024 * 1024
        ),
        cost_estimate=pl.CostEstimate(
            flops=4 * heads * group_rows * keys.shape[0] * LANES * 2,
            bytes_accessed=4 * keys.shape[0] * width,
            transcendentals=heads * group_rows * keys.shape[0],
        ),
        name="attend",
    )(group, queries, keys, values)


def on_device_plain(
    q_latent,
    kv_latent,
    rope_key,
    q_gain,
    kv_gain,
    w_query,
    w_query_rot,
    w_key,
    w_value,
    w_mix_out,
    expert_input,
    ffn_gain,
    expert_ids,
    route_weights,
    w_gate_exp,
    w_up_exp,
    w_down_exp,
):
    tok_rows = q_latent.shape[0]
    tp_count = lax.axis_size("tp")
    expert_count = lax.axis_size("ep")
    slot_count = 3 * tok_rows * TOPK // (2 * expert_count)
    group_rows = tp_count * tok_rows
    heads_here = w_key.shape[1] // NOPE

    gate_all = lax.all_gather(w_gate_exp[0], "tp", axis=0)
    up_all = lax.all_gather(w_up_exp[0], "tp", axis=0)
    down_all = lax.all_gather(w_down_exp[0], "tp", axis=0)

    normed = rms_scale(expert_input, ffn_gain).astype(jnp.bfloat16)
    routed = expert_ids.reshape(-1)
    onehot = (routed[:, None] == jnp.arange(expert_count, dtype=jnp.int32)[None, :]).astype(
        jnp.int32
    )
    slot_number = jnp.sum((jnp.cumsum(onehot, axis=0) - 1) * onehot, axis=-1)
    slot_place = (routed * slot_count + slot_number).reshape(tok_rows, TOPK)
    slot_line = jnp.arange(expert_count * slot_count, dtype=jnp.int32)
    picks = [
        (slot_place[:, route_rank][:, None] == slot_line[None, :]).astype(jnp.bfloat16)
        for route_rank in range(TOPK)
    ]
    dispatch = picks[0]
    for route_rank in range(1, TOPK):
        dispatch = dispatch + picks[route_rank]
    outgoing = lax.dot_general(
        dispatch, normed, (((0,), (0,)), ((), ())), preferred_element_type=jnp.float32
    ).astype(jnp.bfloat16)
    arrived = lax.all_to_all(
        outgoing.reshape(expert_count, slot_count, D), "ep", split_axis=0, concat_axis=0, tiled=True
    )
    rows = arrived.reshape(expert_count * slot_count, D)

    own_rows = jnp.concatenate([kv_latent, rope_key], axis=1)
    ep_rows = lax.all_gather(own_rows, "ep", axis=0, tiled=True)
    column_count = own_rows.shape[1]
    piece_width = column_count // 3 if column_count % 3 == 0 else column_count
    pieces = [
        lax.all_gather(ep_rows[:, first : first + piece_width], "tp", axis=0)
        for first in range(0, column_count, piece_width)
    ]
    kv_rows = (
        jnp.concatenate(pieces, axis=2)
        .reshape(tp_count, expert_count, tok_rows, column_count)
        .transpose(1, 0, 2, 3)
        .reshape(expert_count * group_rows, column_count)
    )
    q_rows = lax.all_gather(q_latent, "tp", axis=0, tiled=True)
    queries = make_queries(q_rows, q_gain, w_query, w_query_rot, heads_here, group_rows)
    keys, values = make_keys(kv_rows, kv_gain, w_key, w_value, heads_here)
    attention = attend(queries, keys, values, heads_here, group_rows)

    total = jnp.zeros((rows.shape[0], D), jnp.float32)
    for block in range(tp_count):
        gate_part = jnp.dot(rows, gate_all[block], preferred_element_type=jnp.float32)
        up_part = jnp.dot(rows, up_all[block], preferred_element_type=jnp.float32)
        hidden = (jax.nn.silu(gate_part) * up_part).astype(jnp.bfloat16)
        part = jnp.dot(hidden, down_all[block], preferred_element_type=jnp.float32)
        total = total + part.astype(jnp.bfloat16).astype(jnp.float32)
    summed = total.astype(jnp.bfloat16)
    results = lax.all_to_all(
        summed.reshape(expert_count, slot_count, D), "ep", split_axis=0, concat_axis=0, tiled=True
    ).reshape(expert_count * slot_count, D)

    partial_out = jnp.dot(attention, w_mix_out, preferred_element_type=jnp.float32).astype(
        jnp.bfloat16
    )
    mixer_out = lax.psum_scatter(partial_out, "tp", scatter_dimension=0, tiled=True)

    fetched = jnp.dot(
        jnp.concatenate(picks, axis=0), results, preferred_element_type=jnp.float32
    ).astype(jnp.bfloat16)
    combined = jnp.zeros((tok_rows, D), jnp.float32)
    for route_rank in range(TOPK):
        piece = fetched[route_rank * tok_rows : (route_rank + 1) * tok_rows].astype(jnp.float32)
        combined = combined + route_weights[:, route_rank : route_rank + 1] * piece
    return (mixer_out, combined.astype(jnp.bfloat16))


MESH = pl.DeviceIdType.MESH


def ring_place(index, count):
    side = index % 2
    line = index // 2
    return line + side * (count - 1 - 2 * line)


def ring_index(place, count):
    side = place // (count // 2)
    line = place + side * (count - 1 - 2 * place)
    return 2 * line + side


def remote(src, dst, send, recv, device):
    return pltpu.make_async_remote_copy(
        src_ref=src, dst_ref=dst, send_sem=send, recv_sem=recv, device_id=device, device_id_type=MESH
    )


def layer_kernel(
    count,
    chunks,
    q_ref,
    kv_ref,
    rope_ref,
    q_gain_ref,
    kv_gain_ref,
    w_query_ref,
    w_rot_ref,
    w_key_ref,
    w_value_ref,
    w_mix_ref,
    cos_ref,
    sin_ref,
    x_ref,
    gain_ref,
    coef_ref,
    gate_ref,
    up_ref,
    down_ref,
    mix_out_ref,
    out_ref,
    q_all,
    wq_cat,
    queries,
    kv_all,
    w_kv,
    kv_now,
    row_max,
    row_acc,
    attended,
    mixed,
    from_core,
    from_cross,
    raw,
    xn,
    wgu,
    wd,
    hid,
    y,
    from_prev,
    from_next,
    coefs,
    coef_col,
    q_send,
    q_recv,
    kvx_sem,
    kvf_send,
    kvf_recv,
    kvb_send,
    kvb_recv,
    kvc_send,
    kvc_recv,
    mix_send,
    mix_recv,
    local_sem,
    coef_send,
    coef_recv,
    fwd_send,
    fwd_recv,
    bwd_send,
    bwd_recv,
    core_send,
    core_recv,
    cross_send,
    cross_recv,
    relay_send,
    relay_recv,
    sum_r_send,
    sum_r_recv,
    sum_l_send,
    sum_l_recv,
):
    bf16, f32 = jnp.bfloat16, jnp.float32
    rows = x_ref.shape[0]
    half_rows = rows // 2
    half = count // 2
    ff = gate_ref.shape[2]
    fh = ff // 2
    width = out_ref.shape[1] // chunks
    group_rows = 4 * rows
    heads = w_key_ref.shape[1] // NOPE
    rank = kv_ref.shape[1]
    head_lanes = heads * LANES
    me = lax.axis_index("ep")
    tp = lax.axis_index("tp")
    place = ring_place(me, count)
    nxt = (ring_index((place + 1) % count, count), tp)
    prv = (ring_index((place + count - 1) % count, count), tp)
    core_peer = (me, tp + 1 - 2 * (tp % 2))
    cross_peer = (me, (tp + 2) % 4)
    diag_peer = (me, 3 - tp)

    barrier = pltpu.get_barrier_semaphore()
    for step in range(1, count):
        pl.semaphore_signal(
            barrier,
            inc=1,
            device_id=(ring_index((place + step) % count, count), tp),
            device_id_type=MESH,
        )
    for peer in (core_peer, cross_peer, diag_peer):
        pl.semaphore_signal(barrier, inc=1, device_id=peer, device_id_type=MESH)

    def rows_of(index):
        return pl.ds(pl.multiple_of(index * rows, rows), rows)

    own_rows, cross_rows = rows_of(tp), rows_of((tp + 2) % 4)

    def scaled(ref, gain):
        floats = ref[...].astype(f32)
        scale = lax.rsqrt(jnp.mean(floats * floats, axis=-1, keepdims=True) + norm_epsilon)
        return (floats * scale * gain[...]).astype(bf16)

    turn_row = lax.broadcasted_iota(jnp.int32, (ROPE, LANES), 0)
    turn_col = lax.broadcasted_iota(jnp.int32, (ROPE, LANES), 1) - NOPE
    straight = (turn_row == turn_col).astype(f32).astype(bf16)
    swapped = (
        ((turn_row == turn_col + ROPE // 2) & (turn_col < ROPE // 2))
        | ((turn_row == turn_col - ROPE // 2) & (turn_col >= ROPE // 2))
    )
    swapped = jnp.where(swapped, 1.0, 0.0).astype(bf16)
    rope = rope_ref[...]
    turned = (
        jnp.dot(rope, straight, preferred_element_type=f32) * cos_ref[own_rows, :]
        + jnp.dot(rope, swapped, preferred_element_type=f32) * sin_ref[own_rows, :]
    )
    lane = lax.broadcasted_iota(jnp.int32, (rows, LANES), 1)
    kv_all[0, own_rows, 0:rank] = scaled(kv_ref, kv_gain_ref)
    kv_all[0, own_rows, rank : rank + LANES] = jnp.where(
        lane == NOPE + ROPE, 1.0, turned
    ).astype(bf16)
    q_all[own_rows, :] = scaled(q_ref, q_gain_ref)
    pl.semaphore_wait(barrier, count + 2)

    sent = []

    def go(copy):
        copy.start()
        sent.append(copy)
        return copy

    def half_of(h):
        return pl.ds(h * half_rows, half_rows)

    part_rows = (own_rows, cross_rows)

    def kv_forward(step, p):
        return remote(
            kv_all.at[step - 1, part_rows[p]],
            kv_all.at[step, part_rows[p]],
            kvf_send.at[step, p],
            kvf_recv.at[step, p],
            nxt,
        )

    def kv_backward(step, p):
        return remote(
            kv_all.at[(count - step + 1) % count, part_rows[p]],
            kv_all.at[count - step, part_rows[p]],
            kvb_send.at[step, p],
            kvb_recv.at[step, p],
            prv,
        )

    def kv_core(slot, p):
        return remote(
            kv_all.at[slot, part_rows[p]],
            kv_all.at[slot, part_rows[p]],
            kvc_send.at[slot, p],
            kvc_recv.at[slot, p],
            core_peer,
        )

    def forward(step, h):
        src = x_ref.at[half_of(h)] if step == 1 else raw.at[step - 1, half_of(h)]
        return remote(
            src, raw.at[step, half_of(h)], fwd_send.at[step, h], fwd_recv.at[step, h], nxt
        )

    def backward(step, h):
        src = x_ref.at[half_of(h)] if step == 1 else raw.at[count - step + 1, half_of(h)]
        return remote(
            src, raw.at[count - step, half_of(h)], bwd_send.at[step, h], bwd_recv.at[step, h], prv
        )

    def piece(i, slot):
        if i < 4:
            return wgu.at[slot, i // 2, :, pl.ds((i % 2) * fh, fh)]
        return wd.at[i - 4, pl.ds(slot * ff, ff)]

    def own_piece(i):
        if i < 4:
            ref = (gate_ref, up_ref)[i % 2]
            return ref.at[0, :, pl.ds((i // 2) * fh, fh)]
        return down_ref.at[0, :, pl.ds((i - 4) * width, width)]

    kvr, ring = {}, {}
    kvr["x"] = go(
        remote(
            kv_all.at[0, own_rows],
            kv_all.at[0, own_rows],
            kvx_sem.at[0],
            kvx_sem.at[1],
            cross_peer,
        )
    )
    kvr["f", 1, 0] = go(kv_forward(1, 0))
    kvr["b", 1, 0] = go(kv_backward(1, 0))
    kvr["c", 0, 0] = go(kv_core(0, 0))
    q_copies = [
        go(remote(q_all.at[own_rows], q_all.at[own_rows], q_send.at[i], q_recv.at[i], peer))
        for i, peer in enumerate((core_peer, cross_peer, diag_peer))
    ]
    to_coefs = [
        go(
            remote(
                coef_ref,
                coefs.at[step],
                coef_send.at[step],
                coef_recv.at[step],
                (ring_index((place + step) % count, count), tp),
            )
        )
        for step in range(1, count)
    ]
    local, to_core, to_cross, relay = [], [], [], []
    for i in range(4 + chunks):
        to_cross.append(
            go(remote(own_piece(i), piece(i, 2), cross_send.at[i], cross_recv.at[i], cross_peer))
        )
        to_core.append(
            go(remote(own_piece(i), piece(i, 1), core_send.at[i], core_recv.at[i], core_peer))
        )
        copy = pltpu.make_async_copy(own_piece(i), piece(i, 0), local_sem.at[i])
        copy.start()
        local.append(copy)

    def pass_on(i):
        to_cross[i].wait_recv()
        relay.append(
            go(remote(piece(i, 2), piece(i, 3), relay_send.at[i], relay_recv.at[i], core_peer))
        )

    order = [0, half]
    for step in range(1, half):
        order += [step, count - step]

    def base(slot):
        return order.index(slot) * rows

    def norm(slot):
        xn[base(slot) : base(slot) + rows, :] = scaled(
            x_ref if slot == 0 else raw.at[slot], gain_ref
        )

    def coefficient(slot):
        source = coef_ref if slot == 0 else coefs.at[slot]
        line = jnp.broadcast_to(source[pl.ds(me, 1), :], (rows, rows))
        row_id = lax.broadcasted_iota(jnp.int32, (rows, rows), 0)
        col_id = lax.broadcasted_iota(jnp.int32, (rows, rows), 1)
        coef_col[base(slot) : base(slot) + rows, :] = jnp.sum(
            jnp.where(row_id == col_id, line, 0.0), axis=-1, keepdims=True
        )

    w_kv[...] = jnp.zeros_like(w_kv)
    for head in range(heads):
        at = head * LANES
        w_kv[0:rank, at : at + NOPE] = w_key_ref[:, head * NOPE : (head + 1) * NOPE]
        at += head_lanes
        w_kv[0:rank, at : at + VD] = w_value_ref[:, head * VD : (head + 1) * VD]
    pass_row = lax.broadcasted_iota(jnp.int32, (LANES, 2 * head_lanes), 0)
    pass_col = lax.broadcasted_iota(jnp.int32, (LANES, 2 * head_lanes), 1)
    as_key = (
        (pass_col < head_lanes)
        & (pass_col % LANES == pass_row)
        & (pass_row >= NOPE)
        & (pass_row < NOPE + ROPE)
    )
    as_one = (pass_col >= head_lanes) & (pass_col % LANES == VD) & (pass_row == NOPE + ROPE)
    w_kv[rank : rank + LANES, :] = jnp.where(as_key | as_one, 1.0, 0.0).astype(bf16)

    kvr["x"].wait_recv()
    kvr["f", 1, 1] = go(kv_forward(1, 1))
    kvr["b", 1, 1] = go(kv_backward(1, 1))
    kvr["c", 0, 1] = go(kv_core(0, 1))
    ring["f", 1, 0] = go(forward(1, 0))
    ring["b", 1, 0] = go(backward(1, 0))

    wq_cat[...] = jnp.zeros_like(wq_cat)
    for head in range(heads):
        at = head * LANES
        turn = head * ROPE
        wq_cat[:, at : at + NOPE] = w_query_ref[:, head * NOPE : (head + 1) * NOPE]
        wq_cat[:, at + NOPE : at + NOPE + ROPE] = w_rot_ref[:, turn : turn + ROPE]
        at += head_lanes + NOPE
        wq_cat[:, at : at + ROPE // 2] = w_rot_ref[:, turn + ROPE // 2 : turn + ROPE]
        wq_cat[:, at + ROPE // 2 : at + ROPE] = w_rot_ref[:, turn : turn + ROPE // 2]

    for copy in q_copies:
        copy.wait_recv()
    both = jnp.dot(q_all[...], wq_cat[...], preferred_element_type=f32)
    for head in range(heads):
        at = head * LANES
        queries[:, at : at + LANES] = (
            both[:, at : at + LANES] * cos_ref[...]
            + both[:, head_lanes + at : head_lanes + at + LANES] * sin_ref[...]
        ).astype(bf16)
    row_max[...] = jnp.full(row_max.shape, masked_score, f32)
    row_acc[...] = jnp.zeros(row_acc.shape, f32)

    log_scale = (NOPE + ROPE) ** (-0.5) * math.log2(math.e)
    chunk = group_rows // 2

    def work(slot, masked):
        kv_now[...] = jnp.dot(
            kv_all[slot], w_kv[...], preferred_element_type=f32
        ).astype(bf16)

        @pl.loop(0, heads // 2)
        def _(pair):
            for sub in range(2):
                head = pair * 2 + sub
                lanes = pl.ds(pl.multiple_of(head * LANES, LANES), LANES)
                value_lanes = pl.ds(pl.multiple_of(head_lanes + head * LANES, LANES), LANES)
                for first in range(0, group_rows, chunk):
                    part = slice(first, first + chunk)
                    scores = lax.dot_general(
                        queries[part, lanes],
                        kv_now[:, lanes],
                        (((1,), (1,)), ((), ())),
                        preferred_element_type=f32,
                    )
                    if masked:
                        row_id = lax.broadcasted_iota(jnp.int32, scores.shape, 0) + first
                        col_id = lax.broadcasted_iota(jnp.int32, scores.shape, 1)
                        scores = jnp.where(
                            col_id // SEG <= row_id // SEG, scores, masked_score
                        )
                    old = row_max[head, part, :]
                    new = jnp.maximum(old, jnp.max(scores, axis=-1, keepdims=True))
                    weights = jnp.exp2((scores - new[:, :1]) * log_scale).astype(bf16)
                    factor = jnp.exp2((old - new) * log_scale)
                    row_max[head, part, :] = new
                    row_acc[head, part, :] = row_acc[head, part, :] * factor + jnp.dot(
                        weights, kv_now[:, value_lanes], preferred_element_type=f32
                    )

    def attend_slot(slot):
        kvr["c", slot, 0].wait_recv()
        kvr["c", slot, 1].wait_recv()
        if slot == 0:
            work(0, True)
        else:

            @pl.when(ring_index((place + count - slot) % count, count) < me)
            def _():
                work(slot, False)

    def kv_step(step):
        for p in range(2):
            if ("f", step, p) in kvr:
                kvr["f", step, p].wait_recv()
                if step + 1 < half or (step + 1 == half and p == 0):
                    kvr["f", step + 1, p] = go(kv_forward(step + 1, p))
                kvr["c", step, p] = go(kv_core(step, p))
            if ("b", step, p) in kvr:
                kvr["b", step, p].wait_recv()
                if step + 1 < half or (step + 1 == half and p == 1):
                    kvr["b", step + 1, p] = go(kv_backward(step + 1, p))
                kvr["c", count - step, p] = go(kv_core(count - step, p))

    def token_step(step, h):
        ring["f", step, h].wait_recv()
        if step + 1 < half or h == 0:
            ring["f", step + 1, h] = go(forward(step + 1, h))
        ring["b", step, h].wait_recv()
        if step + 1 < half or h == 1:
            ring["b", step + 1, h] = go(backward(step + 1, h))

    tile_rows = 2 * rows

    def hidden(slot_from, slot_to, h, tile_from, tile_to):
        @pl.loop(slot_from, slot_to)
        def _(slot):
            @pl.loop(tile_from, tile_to)
            def _(tile):
                part = pl.ds(pl.multiple_of(tile * tile_rows, tile_rows), tile_rows)
                both = jnp.dot(xn[part, :], wgu[slot, h], preferred_element_type=f32)
                gate = both[:, :fh]
                at = pl.ds(pl.multiple_of((slot * 2 + h) * fh, fh), fh)
                hid[part, at] = (gate * jax.nn.sigmoid(gate) * both[:, fh:]).astype(bf16)

    norm(0)
    coefficient(0)
    attend_slot(0)
    kv_step(1)
    ring["f", 1, 1] = go(forward(1, 1))
    ring["b", 1, 1] = go(backward(1, 1))
    for copy in to_coefs:
        copy.wait_recv()
    for slot in range(1, count):
        coefficient(slot)
    attend_slot(1)
    attend_slot(count - 1)
    for i in range(4):
        local[i].wait()
        to_core[i].wait_recv()
    for step in range(2, half + 1):
        kv_step(step)
        token_step(step - 1, 0)
        attend_slot(step)
        token_step(step - 1, 1)
        if step < half:
            attend_slot(count - step)
        norm(step - 1)
        norm(count - step + 1)
        pass_on(step - 2)
        for h in range(2):
            hidden(0, 2, h, step - 1, step)

    for head in range(heads):
        acc = row_acc[head]
        attended[:, head * VD : (head + 1) * VD] = (
            acc[:, :VD] / acc[:, VD : VD + 1]
        ).astype(bf16)

    @pl.loop(0, 4)
    def _(block):
        part = pl.ds(pl.multiple_of(block * rows, rows), rows)
        mixed[block] = jnp.dot(
            attended[part, :], w_mix_ref[...], preferred_element_type=f32
        ).astype(bf16)

    core_tp = tp + 1 - 2 * (tp % 2)
    mixes = [
        go(
            remote(
                mixed.at[core_tp], from_core.at[0], mix_send.at[0], mix_recv.at[0], core_peer
            )
        ),
        go(
            remote(
                mixed.at[3 - tp], from_core.at[1], mix_send.at[1], mix_recv.at[1], core_peer
            )
        ),
    ]

    def add(target, source):
        target[...] = (target[...].astype(f32) + source[...].astype(f32)).astype(bf16)

    def mix_cross():
        mixes[1].wait_recv()
        add(mixed.at[(tp + 2) % 4], from_core.at[1])
        mixes.append(
            go(
                remote(
                    mixed.at[(tp + 2) % 4], from_cross, mix_send.at[2], mix_recv.at[2], cross_peer
                )
            )
        )

    def mix_end():
        mixes[0].wait_recv()
        mixes[2].wait_recv()
        mix_out_ref[...] = (
            mixed[tp].astype(f32) + from_core[0].astype(f32) + from_cross[...].astype(f32)
        ).astype(bf16)

    pair_count = half
    for i in range(2):
        relay[i].wait_recv()
    hidden(2, 4, 0, 1, pair_count)
    ring["f", half, 0].wait_recv()
    ring["b", half, 1].wait_recv()
    norm(half)
    for h in range(2):
        hidden(0, 2, h, 0, 1)
    hidden(2, 4, 0, 0, 1)
    mix_cross()
    while len(relay) < 4:
        pass_on(len(relay))
    for i in range(2, 4):
        relay[i].wait_recv()
    hidden(2, 4, 1, 0, pair_count)

    def down(c):
        pass_on(4 + c)
        local[4 + c].wait()
        to_core[4 + c].wait_recv()
        relay[4 + c].wait_recv()

        @pl.loop(0, pair_count)
        def _(tile):
            part = pl.ds(pl.multiple_of(tile * tile_rows, tile_rows), tile_rows)
            acc = jnp.dot(hid[part, :], wd[c], preferred_element_type=f32)
            y[c, part, :] = (acc * coef_col[part, :]).astype(bf16)

    def block(slot, h=None):
        if h is None:
            return pl.ds(base(slot), rows)
        return pl.ds(base(slot) + h * half_rows, half_rows)

    sums = {}

    def send_sum(c, k, slot_r, slot_l, h_r=None, h_l=None):
        def landing(ref, h):
            return ref.at[c, k] if h is None else ref.at[c, k, half_of(h)]

        sums["r", c, k] = (
            y.at[c, block(slot_r, h_r)],
            landing(from_prev, h_r),
            sum_r_send.at[c, k],
            sum_r_recv.at[c, k],
            nxt,
        )
        sums["l", c, k] = (
            y.at[c, block(slot_l, h_l)],
            landing(from_next, h_l),
            sum_l_send.at[c, k],
            sum_l_recv.at[c, k],
            prv,
        )

    def start_sum(key):
        sums[key] = go(remote(*sums[key]))

    def sum_start(c):
        send_sum(c, 0, half, half, 0, 1)
        start_sum(("r", c, 0))
        start_sum(("l", c, 0))

    def sum_step(c, k):
        send_sum(c, k, half + k, half - k)
        sums["r", c, k - 1].wait_recv()
        if k == 1:
            add(y.at[c, block(half + k, 0)], from_prev.at[c, 0, half_of(0)])
        else:
            add(y.at[c, block(half + k)], from_prev.at[c, k - 1])
        start_sum(("r", c, k))
        sums["l", c, k - 1].wait_recv()
        if k == 1:
            add(y.at[c, block(half - k, 1)], from_next.at[c, 0, half_of(1)])
        else:
            add(y.at[c, block(half - k)], from_next.at[c, k - 1])
        start_sum(("l", c, k))

    def sum_end(c):
        sums["r", c, half - 1].wait_recv()
        sums["l", c, half - 1].wait_recv()
        out_ref[:, c * width : (c + 1) * width] = (
            y[c, block(0), :].astype(f32)
            + from_prev[c, half - 1].astype(f32)
            + from_next[c, half - 1].astype(f32)
        ).astype(bf16)

    for tick in range(chunks + half):
        for c in range(chunks):
            k = tick - c
            if 1 <= k < half:
                sum_step(c, k)
            elif k == half:
                sum_end(c)
        if tick < chunks:
            down(tick)
            sum_start(tick)
        if tick == chunks + 1:
            mix_end()
    for copy in sent:
        copy.wait_send()


def turn_tables(group_rows):
    half_width = ROPE // 2
    frequency = rope_base ** (-jnp.arange(half_width, dtype=jnp.float32) / half_width)
    positions = lax.axis_index("ep") * group_rows + jnp.arange(group_rows, dtype=jnp.int32)
    angles = positions.astype(jnp.float32)[:, None] * jnp.tile(frequency, LANES // half_width)[None, :]
    lane = jnp.arange(LANES, dtype=jnp.int32)[None, :]
    inside = (lane >= NOPE) & (lane < NOPE + ROPE)
    cosine = jnp.where(inside, jnp.cos(angles), jnp.where(lane < NOPE, 1.0, 0.0))
    sine = jnp.where(inside, jnp.sin(angles), 0.0)
    return cosine, jnp.where(lane < NOPE + half_width, -sine, sine)


def coefficients(expert_ids, route_weights, expert_count):
    experts = jnp.arange(expert_count, dtype=jnp.int32)
    named = expert_ids.T[:, None, :] == experts[None, :, None]
    return jnp.sum(jnp.where(named, route_weights.T[:, None, :], 0.0), axis=0)


def on_device_fused(
    q_latent,
    kv_latent,
    rope_key,
    q_gain,
    kv_gain,
    w_query,
    w_query_rot,
    w_key,
    w_value,
    w_mix_out,
    expert_input,
    ffn_gain,
    expert_ids,
    route_weights,
    w_gate_exp,
    w_up_exp,
    w_down_exp,
):
    count = lax.axis_size("ep")
    chunks = 4
    rows, depth = expert_input.shape
    ff = w_gate_exp.shape[2]
    heads = w_key.shape[1] // NOPE
    rank = kv_latent.shape[1]
    q_rank = q_latent.shape[1]
    group_rows = 4 * rows
    half = count // 2
    width = depth // chunks
    pieces = 4 + chunks
    head_lanes = heads * LANES
    kv_width = rank + LANES
    coef = coefficients(expert_ids, route_weights, count)
    cosine, sine = turn_tables(group_rows)
    bf16, f32 = jnp.bfloat16, jnp.float32
    dma = pltpu.SemaphoreType.DMA
    vmem = pl.BlockSpec(memory_space=pltpu.VMEM)
    hbm = pl.BlockSpec(memory_space=pl.ANY)
    return pl.pallas_call(
        functools.partial(layer_kernel, count, chunks),
        out_shape=[jax.ShapeDtypeStruct((rows, depth), bf16)] * 2,
        in_specs=[vmem] * 15 + [hbm] * 3,
        out_specs=[vmem, vmem],
        scratch_shapes=[
            pltpu.VMEM((group_rows, q_rank), bf16),
            pltpu.VMEM((q_rank, 2 * head_lanes), bf16),
            pltpu.VMEM((group_rows, head_lanes), bf16),
            pltpu.VMEM((count, group_rows, kv_width), bf16),
            pltpu.VMEM((kv_width, 2 * head_lanes), bf16),
            pltpu.VMEM((group_rows, 2 * head_lanes), bf16),
            pltpu.VMEM((heads, group_rows, LANES), f32),
            pltpu.VMEM((heads, group_rows, LANES), f32),
            pltpu.VMEM((group_rows, heads * VD), bf16),
            pltpu.VMEM((4, rows, depth), bf16),
            pltpu.VMEM((2, rows, depth), bf16),
            pltpu.VMEM((rows, depth), bf16),
            pltpu.VMEM((count, rows, depth), bf16),
            pltpu.VMEM((count * rows, depth), bf16),
            pltpu.VMEM((4, 2, depth, ff), bf16),
            pltpu.VMEM((chunks, 4 * ff, width), bf16),
            pltpu.VMEM((count * rows, 4 * ff), bf16),
            pltpu.VMEM((chunks, count * rows, width), bf16),
            pltpu.VMEM((chunks, half, rows, width), bf16),
            pltpu.VMEM((chunks, half, rows, width), bf16),
            pltpu.VMEM((count, count, rows), f32),
            pltpu.VMEM((count * rows, 1), f32),
            dma((3,)),
            dma((3,)),
            dma((2,)),
            dma((half + 1, 2)),
            dma((half + 1, 2)),
            dma((half + 1, 2)),
            dma((half + 1, 2)),
            dma((count, 2)),
            dma((count, 2)),
            dma((3,)),
            dma((3,)),
            dma((pieces,)),
            dma((count,)),
            dma((count,)),
            dma((half + 1, 2)),
            dma((half + 1, 2)),
            dma((half + 1, 2)),
            dma((half + 1, 2)),
            dma((pieces,)),
            dma((pieces,)),
            dma((pieces,)),
            dma((pieces,)),
            dma((pieces,)),
            dma((pieces,)),
            dma((chunks, half)),
            dma((chunks, half)),
            dma((chunks, half)),
            dma((chunks, half)),
        ],
        compiler_params=pltpu.CompilerParams(
            collective_id=0, has_side_effects=True, vmem_limit_bytes=63 * 1024 * 1024
        ),
        cost_estimate=pl.CostEstimate(
            flops=6 * count * rows * depth * 4 * ff,
            bytes_accessed=12 * depth * ff * 2,
            transcendentals=count * rows * 4 * ff,
        ),
        name="layer",
    )(
        q_latent,
        kv_latent,
        rope_key,
        q_gain.reshape(1, -1),
        kv_gain.reshape(1, -1),
        w_query,
        w_query_rot,
        w_key,
        w_value,
        w_mix_out,
        cosine,
        sine,
        expert_input,
        ffn_gain.reshape(1, -1),
        coef,
        w_gate_exp,
        w_up_exp,
        w_down_exp,
    )


def fits(mesh):
    ep, tp = mesh.shape["ep"], mesh.shape["tp"]
    return tp == 4 and ep % 2 == 0 and 4 <= ep <= 8


def solution(mesh):
    return jax.shard_map(
        on_device_fused if fits(mesh) else on_device_plain,
        mesh=mesh,
        in_specs=(
            P(("ep", "tp"), None),
            P(("ep", "tp"), None),
            P(("ep", "tp"), None),
            P(),
            P(),
            P(None, "tp"),
            P(None, "tp"),
            P(None, "tp"),
            P(None, "tp"),
            P("tp", None),
            P(("ep", "tp"), None),
            P(),
            P(("ep", "tp"), None),
            P(("ep", "tp"), None),
            P("ep", None, "tp"),
            P("ep", None, "tp"),
            P("ep", "tp", None),
        ),
        out_specs=(P(("ep", "tp"), None), P(("ep", "tp"), None)),
        check_vma=False,
    )
```

profile of v0, /device:TPU:0, one launch (start us, length us, event | category | flops | bytes accessed | tf_op | source)
XLA Modules:
  0.0 138.5 jit_solution(7791803061431579879)
XLA Ops:
  0.7 0.0 copy-start.2
  0.7 0.0 copy-start.3
  0.7 0.0 copy-start.1
  0.7 0.1 mul.20
  0.8 0.5 copy-done.2
  1.4 0.0 copy-done.3
  1.4 0.6 select_reduce_fusion.coef_ref
  2.0 0.0 copy-done.1
  2.0 0.7 copy.20.rope_ref
  2.7 1.8 %negate_select_fusion = (f32[512,128]{1,0:T(8,128)}, f32[512,128]{1,0:T(8,128)}) fusion(f32[128]{0:T(128)S(1)} %mul.20, f32[512]{0:T(512)S(1)} %add_convert_fusion, pred[128]{0:T(512)(128)(4,1)S(1)} %get-tuple-element.5, pred[128]{0:T(512)(128)(4,1)S(1)} %get-tuple-element.4, f32[128]{0:T(128)S(1)} %compare_select_fusion), kind=kLoop, calls=%fused_computation | loop fusion | flops 327680 | bytes 527616 | tf_op jit(solution)/shard_map/jit(_where)/select_n | solution.py:877
  4.5 131.2 %layer.1 = (bf16[128,2048]{1,0:T(8,128)(2,1)}, bf16[128,2048]{1,0:T(8,128)(2,1)}) custom-call(bf16[128,512]{1,0:T(8,128)(2,1)} %q_ref.1, bf16[128,256]{1,0:T(8,128)(2,1)} %kv_ref.1, bf16[128,32]{1,0:T(8,128)(2,1)} %copy.20.rope_ref, f32[1,512]{1,0:T(1,128)} %bitcast.8, f32[1,256]{1,0:T(1,128)} %bitcast.9, bf16[512,256]{1,0:T(8,128)(2,1)} %w_query_ref.1, ...), custom_call_target="tpu_custom_call" | custom-call | flops 12884901888 | bytes 12582912 | tf_op jit(solution)/shard_map/layer/pallas_call | solution.py:924
  135.7 0.0 copy-start
  135.7 1.9 %copy.23 = bf16[128,2048]{1,0:T(8,128)(2,1)} copy(bf16[128,2048]{1,0:T(8,128)(2,1)} %get-tuple-element.8) | data formatting | bytes 1048576
  137.7 0.0 copy-done
  137.7 0.8 copy.24
  (5 shorter events, 0.0 us)
Async XLA Ops:
  0.7 0.7 copy-start.2
  0.7 0.7 copy-start.3
  0.7 1.3 copy-start.1
  135.7 2.0 %copy-start = (bf16[128,2048]{1,0:T(8,128)(2,1)S(1)}, bf16[128,2048]{1,0:T(8,128)(2,1)}, u32[]{:S(2)}) copy-start(bf16[128,2048]{1,0:T(8,128)(2,1)} %get-tuple-element.9) | copy-start | bytes 1572868
where the time goes:
time: 139 us; the launch traced here: 138 us
  Pallas kernels  131 us (94%)
  local copies, waits for them, and re-layouts  4.11 us (3%)
  other arithmetic  2.45 us (2%)
    pallas_call x1, Pallas kernels, on_device_fused(): pl.pallas_call(functools.partial(layer_kernel, count, chunks), out_shape=...  131 us
    unnamed x11, local copies, waits for them, and re-layouts  4.03 us

commit v1 on v0

--- a/solution.py
+++ b/solution.py
@@ -3,6 +3,7 @@
 
 import jax
 import jax.numpy as jnp
+import numpy as np
 from jax import lax
 from jax.experimental import pallas as pl
 from jax.experimental.pallas import tpu as pltpu
@@ -272,6 +273,7 @@
 
 
 MESH = pl.DeviceIdType.MESH
+VR = VD + 16
 
 
 def ring_place(index, count):
@@ -290,6 +292,41 @@
     return pltpu.make_async_remote_copy(
         src_ref=src, dst_ref=dst, send_sem=send, recv_sem=recv, device_id=device, device_id_type=MESH
     )
+
+
+def sum_plan(chunks, half):
+    block = 11.2 / chunks
+    lag = 1.7
+    now, link = 0.0, 0.0
+    arrive, plan = {}, []
+    downs, side = 0, [("cross", 12.0), ("close", 34.0)]
+    while downs < chunks or arrive or side:
+        ready = sorted((k, c) for (c, k), at in arrive.items() if at <= now)
+        can_down = downs < chunks and downs * 22.4 / chunks <= now
+        if side and side[0][1] <= now:
+            plan.append((side.pop(0)[0], 0, 0))
+        elif can_down and (link > now + 0.4 or not ready):
+            plan.append(("down", downs, 0))
+            link = max(link, now + 0.4) + block / 2
+            arrive[downs, 1] = link + lag
+            now += 10.0 / chunks
+            downs += 1
+        elif ready:
+            k, c = ready[0]
+            del arrive[c, k]
+            now += 0.1
+            if k < half:
+                plan.append(("step", c, k))
+                link = max(link, now) + block
+                arrive[c, k + 1] = link + lag
+            else:
+                plan.append(("end", c, k))
+        else:
+            times = list(arrive.values()) + [at for _, at in side]
+            if downs < chunks:
+                times.append(downs * 22.4 / chunks)
+            now = max(now + 0.01, min(times))
+    return plan
 
 
 def layer_kernel(
@@ -305,22 +342,35 @@
     w_key_ref,
     w_value_ref,
     w_mix_ref,
-    cos_ref,
-    sin_ref,
+    freq_ref,
     x_ref,
     gain_ref,
-    coef_ref,
+    ids_ref,
+    route_ref,
     gate_ref,
     up_ref,
     down_ref,
     mix_out_ref,
     out_ref,
+    x_now,
+    w_query_now,
+    w_rot_now,
+    w_key_now,
+    w_value_now,
+    w_mix_now,
+    mix_stage,
+    out_stage,
+    cos_ref,
+    sin_ref,
+    coef_ref,
     q_all,
     wq_cat,
     queries,
     kv_all,
     w_kv,
-    kv_now,
+    w_vt,
+    k_now,
+    v_now,
     row_max,
     row_acc,
     attended,
@@ -348,6 +398,8 @@
     kvc_recv,
     mix_send,
     mix_recv,
+    in_sem,
+    out_sem,
     local_sem,
     coef_send,
     coef_recv,
@@ -384,7 +436,6 @@
     prv = (ring_index((place + count - 1) % count, count), tp)
     core_peer = (me, tp + 1 - 2 * (tp % 2))
     cross_peer = (me, (tp + 2) % 4)
-    diag_peer = (me, 3 - tp)
 
     barrier = pltpu.get_barrier_semaphore()
     for step in range(1, count):
@@ -394,8 +445,22 @@
             device_id=(ring_index((place + step) % count, count), tp),
             device_id_type=MESH,
         )
-    for peer in (core_peer, cross_peer, diag_peer):
+    for peer in (core_peer, cross_peer):
         pl.semaphore_signal(barrier, inc=1, device_id=peer, device_id_type=MESH)
+
+    inputs = []
+    for i, (src, dst) in enumerate(
+        (
+            (x_ref, x_now),
+            (w_key_ref, w_key_now),
+            (w_value_ref, w_value_now),
+            (w_query_ref, w_query_now),
+            (w_rot_ref, w_rot_now),
+            (w_mix_ref, w_mix_now),
+        )
+    ):
+        inputs.append(pltpu.make_async_copy(src, dst, in_sem.at[i]))
+        inputs[-1].start()
 
     def rows_of(index):
         return pl.ds(pl.multiple_of(index * rows, rows), rows)
@@ -406,6 +471,17 @@
         floats = ref[...].astype(f32)
         scale = lax.rsqrt(jnp.mean(floats * floats, axis=-1, keepdims=True) + norm_epsilon)
         return (floats * scale * gain[...]).astype(bf16)
+
+    def turn_table(first, size):
+        lane = lax.broadcasted_iota(jnp.int32, (size, LANES), 1)
+        row = lax.broadcasted_iota(jnp.int32, (size, LANES), 0)
+        angle = (me * group_rows + first + row).astype(f32) * freq_ref[...]
+        inside = (lane >= NOPE) & (lane < NOPE + ROPE)
+        sine = jnp.where(inside, jnp.sin(angle), 0.0)
+        return (
+            jnp.where(inside, jnp.cos(angle), jnp.where(lane < NOPE, 1.0, 0.0)),
+            jnp.where(lane < NOPE + ROPE // 2, -sine, sine),
+        )
 
     turn_row = lax.broadcasted_iota(jnp.int32, (ROPE, LANES), 0)
     turn_col = lax.broadcasted_iota(jnp.int32, (ROPE, LANES), 1) - NOPE
@@ -416,9 +492,11 @@
     )
     swapped = jnp.where(swapped, 1.0, 0.0).astype(bf16)
     rope = rope_ref[...]
+    own_cos, own_sin = turn_table(tp * rows, rows)
+    by_column = (((0,), (0,)), ((), ()))
     turned = (
-        jnp.dot(rope, straight, preferred_element_type=f32) * cos_ref[own_rows, :]
-        + jnp.dot(rope, swapped, preferred_element_type=f32) * sin_ref[own_rows, :]
+        lax.dot_general(rope, straight, by_column, preferred_element_type=f32) * own_cos
+        + lax.dot_general(rope, swapped, by_column, preferred_element_type=f32) * own_sin
     )
     lane = lax.broadcasted_iota(jnp.int32, (rows, LANES), 1)
     kv_all[0, own_rows, 0:rank] = scaled(kv_ref, kv_gain_ref)
@@ -426,13 +504,15 @@
         lane == NOPE + ROPE, 1.0, turned
     ).astype(bf16)
     q_all[own_rows, :] = scaled(q_ref, q_gain_ref)
-    pl.semaphore_wait(barrier, count + 2)
-
-    sent = []
+    expert_id = lax.broadcasted_iota(jnp.int32, (count, rows), 0)
+    coef = jnp.zeros((count, rows), f32)
+    for k in range(TOPK):
+        coef += jnp.where(ids_ref[k : k + 1, :] == expert_id, route_ref[k : k + 1, :], 0.0)
+    coef_ref[...] = coef
+    pl.semaphore_wait(barrier, count + 1)
 
     def go(copy):
         copy.start()
-        sent.append(copy)
         return copy
 
     def half_of(h):
@@ -444,8 +524,8 @@
         return remote(
             kv_all.at[step - 1, part_rows[p]],
             kv_all.at[step, part_rows[p]],
-            kvf_send.at[step, p],
-            kvf_recv.at[step, p],
+            kvf_send,
+            kvf_recv.at[step - 1, p],
             nxt,
         )
 
@@ -453,8 +533,8 @@
         return remote(
             kv_all.at[(count - step + 1) % count, part_rows[p]],
             kv_all.at[count - step, part_rows[p]],
-            kvb_send.at[step, p],
-            kvb_recv.at[step, p],
+            kvb_send,
+            kvb_recv.at[step - 1, p],
             prv,
         )
 
@@ -462,7 +542,7 @@
         return remote(
             kv_all.at[slot, part_rows[p]],
             kv_all.at[slot, part_rows[p]],
-            kvc_send.at[slot, p],
+            kvc_send,
             kvc_recv.at[slot, p],
             core_peer,
         )
@@ -470,13 +550,13 @@
     def forward(step, h):
         src = x_ref.at[half_of(h)] if step == 1 else raw.at[step - 1, half_of(h)]
         return remote(
-            src, raw.at[step, half_of(h)], fwd_send.at[step, h], fwd_recv.at[step, h], nxt
+            src, raw.at[step, half_of(h)], fwd_send, fwd_recv.at[step - 1, h], nxt
         )
 
     def backward(step, h):
         src = x_ref.at[half_of(h)] if step == 1 else raw.at[count - step + 1, half_of(h)]
         return remote(
-            src, raw.at[count - step, half_of(h)], bwd_send.at[step, h], bwd_recv.at[step, h], prv
+            src, raw.at[count - step, half_of(h)], bwd_send, bwd_recv.at[step - 1, h], prv
         )
 
     def piece(i, slot):
@@ -505,15 +585,17 @@
     kvr["c", 0, 0] = go(kv_core(0, 0))
     q_copies = [
         go(remote(q_all.at[own_rows], q_all.at[own_rows], q_send.at[i], q_recv.at[i], peer))
-        for i, peer in enumerate((core_peer, cross_peer, diag_peer))
+        for i, peer in enumerate((core_peer, cross_peer))
     ]
+    ring["f", 1, 0] = go(forward(1, 0))
+    ring["b", 1, 1] = go(backward(1, 1))
     to_coefs = [
         go(
             remote(
                 coef_ref,
                 coefs.at[step],
-                coef_send.at[step],
-                coef_recv.at[step],
+                coef_send,
+                coef_recv,
                 (ring_index((place + step) % count, count), tp),
             )
         )
@@ -522,10 +604,10 @@
     local, to_core, to_cross, relay = [], [], [], []
     for i in range(4 + chunks):
         to_cross.append(
-            go(remote(own_piece(i), piece(i, 2), cross_send.at[i], cross_recv.at[i], cross_peer))
+            go(remote(own_piece(i), piece(i, 2), cross_send, cross_recv.at[i], cross_peer))
         )
         to_core.append(
-            go(remote(own_piece(i), piece(i, 1), core_send.at[i], core_recv.at[i], core_peer))
+            go(remote(own_piece(i), piece(i, 1), core_send, core_recv.at[i], core_peer))
         )
         copy = pltpu.make_async_copy(own_piece(i), piece(i, 0), local_sem.at[i])
         copy.start()
@@ -534,7 +616,7 @@
     def pass_on(i):
         to_cross[i].wait_recv()
         relay.append(
-            go(remote(piece(i, 2), piece(i, 3), relay_send.at[i], relay_recv.at[i], core_peer))
+            go(remote(piece(i, 2), piece(i, 3), relay_send, relay_recv.at[i], core_peer))
         )
 
     order = [0, half]
@@ -546,7 +628,7 @@
 
     def norm(slot):
         xn[base(slot) : base(slot) + rows, :] = scaled(
-            x_ref if slot == 0 else raw.at[slot], gain_ref
+            x_now if slot == 0 else raw.at[slot], gain_ref
         )
 
     def coefficient(slot):
@@ -559,87 +641,100 @@
         )
 
     w_kv[...] = jnp.zeros_like(w_kv)
+    inputs[1].wait()
     for head in range(heads):
         at = head * LANES
-        w_kv[0:rank, at : at + NOPE] = w_key_ref[:, head * NOPE : (head + 1) * NOPE]
-        at += head_lanes
-        w_kv[0:rank, at : at + VD] = w_value_ref[:, head * VD : (head + 1) * VD]
-    pass_row = lax.broadcasted_iota(jnp.int32, (LANES, 2 * head_lanes), 0)
-    pass_col = lax.broadcasted_iota(jnp.int32, (LANES, 2 * head_lanes), 1)
+        w_kv[0:rank, at : at + NOPE] = w_key_now[:, head * NOPE : (head + 1) * NOPE]
+    pass_row = lax.broadcasted_iota(jnp.int32, (LANES, head_lanes), 0)
+    pass_col = lax.broadcasted_iota(jnp.int32, (LANES, head_lanes), 1)
     as_key = (
-        (pass_col < head_lanes)
-        & (pass_col % LANES == pass_row)
-        & (pass_row >= NOPE)
-        & (pass_row < NOPE + ROPE)
-    )
-    as_one = (pass_col >= head_lanes) & (pass_col % LANES == VD) & (pass_row == NOPE + ROPE)
-    w_kv[rank : rank + LANES, :] = jnp.where(as_key | as_one, 1.0, 0.0).astype(bf16)
+        (pass_col % LANES == pass_row) & (pass_row >= NOPE) & (pass_row < NOPE + ROPE)
+    )
+    w_kv[rank : rank + LANES, :] = jnp.where(as_key, 1.0, 0.0).astype(bf16)
 
     kvr["x"].wait_recv()
     kvr["f", 1, 1] = go(kv_forward(1, 1))
     kvr["b", 1, 1] = go(kv_backward(1, 1))
     kvr["c", 0, 1] = go(kv_core(0, 1))
-    ring["f", 1, 0] = go(forward(1, 0))
-    ring["b", 1, 0] = go(backward(1, 0))
-
+
+    cos_ref[...], sin_ref[...] = turn_table(0, group_rows)
     wq_cat[...] = jnp.zeros_like(wq_cat)
+    inputs[3].wait()
+    inputs[4].wait()
     for head in range(heads):
         at = head * LANES
         turn = head * ROPE
-        wq_cat[:, at : at + NOPE] = w_query_ref[:, head * NOPE : (head + 1) * NOPE]
-        wq_cat[:, at + NOPE : at + NOPE + ROPE] = w_rot_ref[:, turn : turn + ROPE]
+        wq_cat[:, at : at + NOPE] = w_query_now[:, head * NOPE : (head + 1) * NOPE]
+        wq_cat[:, at + NOPE : at + NOPE + ROPE] = w_rot_now[:, turn : turn + ROPE]
         at += head_lanes + NOPE
-        wq_cat[:, at : at + ROPE // 2] = w_rot_ref[:, turn + ROPE // 2 : turn + ROPE]
-        wq_cat[:, at + ROPE // 2 : at + ROPE] = w_rot_ref[:, turn : turn + ROPE // 2]
-
-    for copy in q_copies:
-        copy.wait_recv()
-    both = jnp.dot(q_all[...], wq_cat[...], preferred_element_type=f32)
+        wq_cat[:, at : at + ROPE // 2] = w_rot_now[:, turn + ROPE // 2 : turn + ROPE]
+        wq_cat[:, at + ROPE // 2 : at + ROPE] = w_rot_now[:, turn : turn + ROPE // 2]
+
+    inputs[2].wait()
+    flipped = jnp.transpose(w_value_now[...].astype(f32)).astype(bf16)
+    one_row = lax.broadcasted_iota(jnp.int32, (VR, rank + LANES), 0)
+    one_col = lax.broadcasted_iota(jnp.int32, (VR, rank + LANES), 1)
+    ones = ((one_row == VD) & (one_col == rank + NOPE + ROPE)).astype(f32).astype(bf16)
     for head in range(heads):
-        at = head * LANES
-        queries[:, at : at + LANES] = (
-            both[:, at : at + LANES] * cos_ref[...]
-            + both[:, head_lanes + at : head_lanes + at + LANES] * sin_ref[...]
-        ).astype(bf16)
+        w_vt[head * VR : (head + 1) * VR, :] = ones
+        w_vt[head * VR : head * VR + VD, 0:rank] = flipped[head * VD : (head + 1) * VD, :]
+    inputs[0].wait()
+    norm(0)
+    coefficient(0)
     row_max[...] = jnp.full(row_max.shape, masked_score, f32)
     row_acc[...] = jnp.zeros(row_acc.shape, f32)
+    q_copies[1].wait_recv()
+    q_copies.append(
+        go(
+            remote(
+                q_all.at[cross_rows], q_all.at[cross_rows], q_send.at[2], q_recv.at[2], core_peer
+            )
+        )
+    )
+
+    def make_queries_here():
+        q_copies[0].wait_recv()
+        q_copies[2].wait_recv()
+        both = jnp.dot(q_all[...], wq_cat[...], preferred_element_type=f32)
+        for head in range(heads):
+            at = head * LANES
+            queries[:, at : at + LANES] = (
+                both[:, at : at + LANES] * cos_ref[...]
+                + both[:, head_lanes + at : head_lanes + at + LANES] * sin_ref[...]
+            ).astype(bf16)
 
     log_scale = (NOPE + ROPE) ** (-0.5) * math.log2(math.e)
-    chunk = group_rows // 2
 
     def work(slot, masked):
-        kv_now[...] = jnp.dot(
-            kv_all[slot], w_kv[...], preferred_element_type=f32
-        ).astype(bf16)
+        k_now[...] = jnp.dot(kv_all[slot], w_kv[...], preferred_element_type=f32).astype(bf16)
+        turned_values = lax.dot_general(
+            w_vt[...], kv_all[slot], (((1,), (1,)), ((), ())), preferred_element_type=f32
+        )
+        v_now[...] = turned_values.astype(bf16).reshape(heads, VR, group_rows)
 
         @pl.loop(0, heads // 2)
         def _(pair):
             for sub in range(2):
                 head = pair * 2 + sub
                 lanes = pl.ds(pl.multiple_of(head * LANES, LANES), LANES)
-                value_lanes = pl.ds(pl.multiple_of(head_lanes + head * LANES, LANES), LANES)
-                for first in range(0, group_rows, chunk):
-                    part = slice(first, first + chunk)
-                    scores = lax.dot_general(
-                        queries[part, lanes],
-                        kv_now[:, lanes],
-                        (((1,), (1,)), ((), ())),
-                        preferred_element_type=f32,
-                    )
-                    if masked:
-                        row_id = lax.broadcasted_iota(jnp.int32, scores.shape, 0) + first
-                        col_id = lax.broadcasted_iota(jnp.int32, scores.shape, 1)
-                        scores = jnp.where(
-                            col_id // SEG <= row_id // SEG, scores, masked_score
-                        )
-                    old = row_max[head, part, :]
-                    new = jnp.maximum(old, jnp.max(scores, axis=-1, keepdims=True))
-                    weights = jnp.exp2((scores - new[:, :1]) * log_scale).astype(bf16)
-                    factor = jnp.exp2((old - new) * log_scale)
-                    row_max[head, part, :] = new
-                    row_acc[head, part, :] = row_acc[head, part, :] * factor + jnp.dot(
-                        weights, kv_now[:, value_lanes], preferred_element_type=f32
-                    )
+                scores = lax.dot_general(
+                    k_now[:, lanes],
+                    queries[:, lanes],
+                    (((1,), (1,)), ((), ())),
+                    preferred_element_type=f32,
+                )
+                if masked:
+                    key_id = lax.broadcasted_iota(jnp.int32, scores.shape, 0)
+                    query_id = lax.broadcasted_iota(jnp.int32, scores.shape, 1)
+                    scores = jnp.where(key_id // SEG <= query_id // SEG, scores, masked_score)
+                old = row_max[head]
+                new = jnp.maximum(old, jnp.max(scores, axis=0, keepdims=True))
+                weights = jnp.exp2((scores - new) * log_scale).astype(bf16)
+                factor = jnp.exp2((old - new) * log_scale)
+                row_max[head] = new
+                row_acc[head] = row_acc[head] * factor + jnp.dot(
+                    v_now[head], weights, preferred_element_type=f32
+                )
 
     def attend_slot(slot):
         kvr["c", slot, 0].wait_recv()
@@ -652,101 +747,84 @@
             def _():
                 work(slot, False)
 
-    def kv_step(step):
-        for p in range(2):
-            if ("f", step, p) in kvr:
-                kvr["f", step, p].wait_recv()
-                if step + 1 < half or (step + 1 == half and p == 0):
-                    kvr["f", step + 1, p] = go(kv_forward(step + 1, p))
-                kvr["c", step, p] = go(kv_core(step, p))
-            if ("b", step, p) in kvr:
-                kvr["b", step, p].wait_recv()
-                if step + 1 < half or (step + 1 == half and p == 1):
-                    kvr["b", step + 1, p] = go(kv_backward(step + 1, p))
-                kvr["c", count - step, p] = go(kv_core(count - step, p))
-
-    def token_step(step, h):
-        ring["f", step, h].wait_recv()
-        if step + 1 < half or h == 0:
-            ring["f", step + 1, h] = go(forward(step + 1, h))
-        ring["b", step, h].wait_recv()
-        if step + 1 < half or h == 1:
-            ring["b", step + 1, h] = go(backward(step + 1, h))
+    def kv_step(step, p):
+        if step < half or p == 0:
+            kvr["f", step, p].wait_recv()
+            if step + 1 < half or (step + 1 == half and p == 0):
+                kvr["f", step + 1, p] = go(kv_forward(step + 1, p))
+            kvr["c", step, p] = go(kv_core(step, p))
+        if step < half or p == 1:
+            kvr["b", step, p].wait_recv()
+            if step + 1 < half or (step + 1 == half and p == 1):
+                kvr["b", step + 1, p] = go(kv_backward(step + 1, p))
+            kvr["c", count - step, p] = go(kv_core(count - step, p))
+
+    def token_wait(step, i):
+        ring["f", step, i].wait_recv()
+        ring["b", step, 1 - i].wait_recv()
+
+    def token_pass(step, i):
+        if step + 1 < half or i == 0:
+            ring["f", step + 1, i] = go(forward(step + 1, i))
+            ring["b", step + 1, 1 - i] = go(backward(step + 1, 1 - i))
+
+    def token_step(step, i):
+        token_wait(step, i)
+        token_pass(step, i)
 
     tile_rows = 2 * rows
 
-    def hidden(slot_from, slot_to, h, tile_from, tile_to):
+    def hidden(slot_from, slot_to, halves, first, size, tiles=1):
         @pl.loop(slot_from, slot_to)
         def _(slot):
-            @pl.loop(tile_from, tile_to)
+            @pl.loop(0, tiles)
             def _(tile):
-                part = pl.ds(pl.multiple_of(tile * tile_rows, tile_rows), tile_rows)
-                both = jnp.dot(xn[part, :], wgu[slot, h], preferred_element_type=f32)
-                gate = both[:, :fh]
-                at = pl.ds(pl.multiple_of((slot * 2 + h) * fh, fh), fh)
-                hid[part, at] = (gate * jax.nn.sigmoid(gate) * both[:, fh:]).astype(bf16)
-
-    norm(0)
-    coefficient(0)
-    attend_slot(0)
-    kv_step(1)
-    ring["f", 1, 1] = go(forward(1, 1))
-    ring["b", 1, 1] = go(backward(1, 1))
-    for copy in to_coefs:
-        copy.wait_recv()
-    for slot in range(1, count):
-        coefficient(slot)
-    attend_slot(1)
-    attend_slot(count - 1)
-    for i in range(4):
-        local[i].wait()
-        to_core[i].wait_recv()
-    for step in range(2, half + 1):
-        kv_step(step)
-        token_step(step - 1, 0)
-        attend_slot(step)
-        token_step(step - 1, 1)
-        if step < half:
-            attend_slot(count - step)
-        norm(step - 1)
-        norm(count - step + 1)
-        pass_on(step - 2)
-        for h in range(2):
-            hidden(0, 2, h, step - 1, step)
-
-    for head in range(heads):
-        acc = row_acc[head]
-        attended[:, head * VD : (head + 1) * VD] = (
-            acc[:, :VD] / acc[:, VD : VD + 1]
-        ).astype(bf16)
-
-    @pl.loop(0, 4)
-    def _(block):
-        part = pl.ds(pl.multiple_of(block * rows, rows), rows)
-        mixed[block] = jnp.dot(
-            attended[part, :], w_mix_ref[...], preferred_element_type=f32
-        ).astype(bf16)
-
-    core_tp = tp + 1 - 2 * (tp % 2)
-    mixes = [
-        go(
-            remote(
-                mixed.at[core_tp], from_core.at[0], mix_send.at[0], mix_recv.at[0], core_peer
+                part = pl.ds(pl.multiple_of(first + tile * size, rows), size)
+                for h in halves:
+                    both = jnp.dot(xn[part, :], wgu[slot, h], preferred_element_type=f32)
+                    gate = both[:, :fh]
+                    at = pl.ds(pl.multiple_of((slot * 2 + h) * fh, fh), fh)
+                    hid[part, at] = (gate * jax.nn.sigmoid(gate) * both[:, fh:]).astype(bf16)
+
+    def pair_norm(step):
+        norm(step)
+        norm(count - step)
+
+    def pair_first(step):
+        return base(step)
+
+    mixes = []
+
+    def mix_start():
+        for head in range(heads):
+            acc = row_acc[head]
+            attended[head * VD : (head + 1) * VD, :] = (
+                acc[:VD, :] / acc[VD : VD + 1, :]
+            ).astype(bf16)
+        inputs[5].wait()
+
+        @pl.loop(0, 4)
+        def _(block):
+            part = pl.ds(pl.multiple_of(block * rows, rows), rows)
+            mixed[block] = lax.dot_general(
+                attended[:, part], w_mix_now[...], by_column, preferred_element_type=f32
+            ).astype(bf16)
+
+        for i, index in enumerate((3 - tp, tp + 1 - 2 * (tp % 2))):
+            mixes.append(
+                go(
+                    remote(
+                        mixed.at[index], from_core.at[i], mix_send.at[i], mix_recv.at[i], core_peer
+                    )
+                )
             )
-        ),
-        go(
-            remote(
-                mixed.at[3 - tp], from_core.at[1], mix_send.at[1], mix_recv.at[1], core_peer
-            )
-        ),
-    ]
 
     def add(target, source):
         target[...] = (target[...].astype(f32) + source[...].astype(f32)).astype(bf16)
 
     def mix_cross():
-        mixes[1].wait_recv()
-        add(mixed.at[(tp + 2) % 4], from_core.at[1])
+        mixes[0].wait_recv()
+        add(mixed.at[(tp + 2) % 4], from_core.at[0])
         mixes.append(
             go(
                 remote(
@@ -755,41 +833,33 @@
             )
         )
 
+    outs = []
+
     def mix_end():
-        mixes[0].wait_recv()
+        mixes[1].wait_recv()
         mixes[2].wait_recv()
-        mix_out_ref[...] = (
-            mixed[tp].astype(f32) + from_core[0].astype(f32) + from_cross[...].astype(f32)
+        mix_stage[...] = (
+            mixed[tp].astype(f32) + from_core[1].astype(f32) + from_cross[...].astype(f32)
         ).astype(bf16)
-
-    pair_count = half
-    for i in range(2):
-        relay[i].wait_recv()
-    hidden(2, 4, 0, 1, pair_count)
-    ring["f", half, 0].wait_recv()
-    ring["b", half, 1].wait_recv()
-    norm(half)
-    for h in range(2):
-        hidden(0, 2, h, 0, 1)
-    hidden(2, 4, 0, 0, 1)
-    mix_cross()
-    while len(relay) < 4:
-        pass_on(len(relay))
-    for i in range(2, 4):
-        relay[i].wait_recv()
-    hidden(2, 4, 1, 0, pair_count)
+        outs.append(pltpu.make_async_copy(mix_stage, mix_out_ref, out_sem.at[chunks]))
+        outs[-1].start()
 
     def down(c):
-        pass_on(4 + c)
         local[4 + c].wait()
         to_core[4 + c].wait_recv()
         relay[4 + c].wait_recv()
 
-        @pl.loop(0, pair_count)
-        def _(tile):
-            part = pl.ds(pl.multiple_of(tile * tile_rows, tile_rows), tile_rows)
+        def tile(pair):
+            part = pl.ds(pl.multiple_of(pair * tile_rows, tile_rows), tile_rows)
             acc = jnp.dot(hid[part, :], wd[c], preferred_element_type=f32)
             y[c, part, :] = (acc * coef_col[part, :]).astype(bf16)
+
+        tile(0)
+        sum_start(c)
+
+        @pl.loop(1, half)
+        def _(back):
+            tile(half - back)
 
     def block(slot, h=None):
         if h is None:
@@ -805,14 +875,14 @@
         sums["r", c, k] = (
             y.at[c, block(slot_r, h_r)],
             landing(from_prev, h_r),
-            sum_r_send.at[c, k],
+            sum_r_send,
             sum_r_recv.at[c, k],
             nxt,
         )
         sums["l", c, k] = (
             y.at[c, block(slot_l, h_l)],
             landing(from_next, h_l),
-            sum_l_send.at[c, k],
+            sum_l_send,
             sum_l_recv.at[c, k],
             prv,
         )
@@ -843,44 +913,122 @@
     def sum_end(c):
         sums["r", c, half - 1].wait_recv()
         sums["l", c, half - 1].wait_recv()
-        out_ref[:, c * width : (c + 1) * width] = (
+        columns = slice(c * width, (c + 1) * width)
+        out_stage[:, columns] = (
             y[c, block(0), :].astype(f32)
             + from_prev[c, half - 1].astype(f32)
             + from_next[c, half - 1].astype(f32)
         ).astype(bf16)
-
-    for tick in range(chunks + half):
-        for c in range(chunks):
-            k = tick - c
-            if 1 <= k < half:
-                sum_step(c, k)
-            elif k == half:
-                sum_end(c)
-        if tick < chunks:
-            down(tick)
-            sum_start(tick)
-        if tick == chunks + 1:
+        outs.append(
+            pltpu.make_async_copy(
+                out_stage.at[:, pl.ds(c * width, width)],
+                out_ref.at[:, pl.ds(c * width, width)],
+                out_sem.at[c],
+            )
+        )
+        outs[-1].start()
+
+    everything = (0, 1)
+    for i in range(4):
+        local[i].wait()
+        to_core[i].wait_recv()
+    kv_step(1, 0)
+    ring["f", 1, 1] = go(forward(1, 1))
+    ring["b", 1, 0] = go(backward(1, 0))
+    hidden(0, 2, everything, base(0), rows)
+    make_queries_here()
+    attend_slot(0)
+    kv_step(1, 1)
+    attend_slot(1)
+    kv_step(2, 0)
+    token_step(1, 0)
+    attend_slot(count - 1)
+    remote(coefs.at[1:], coefs.at[1:], coef_send, coef_recv, nxt).wait_recv()
+    for slot in range(1, count):
+        coefficient(slot)
+
+    token_wait(1, 1)
+    pair_norm(1)
+    pass_on(0)
+    hidden(0, 2, everything, base(1), tile_rows)
+    kv_step(2, 1)
+    token_pass(1, 1)
+    attend_slot(2)
+    kv_step(3, 0)
+    attend_slot(count - 2)
+    token_step(2, 0)
+    pass_on(1)
+    kv_step(3, 1)
+    for i in range(2):
+        relay[i].wait_recv()
+    hidden(2, 4, (0,), base(0), rows)
+    hidden(2, 4, (0,), base(1), tile_rows)
+    attend_slot(3)
+    attend_slot(count - 3)
+    token_step(2, 1)
+    pair_norm(2)
+    hidden(0, 2, everything, base(2), tile_rows)
+    kv_step(4, 0)
+    kv_step(4, 1)
+    pass_on(2)
+    hidden(2, 4, (0,), base(2), tile_rows)
+    token_step(3, 0)
+    attend_slot(4)
+    mix_start()
+    token_step(3, 1)
+    pair_norm(3)
+    hidden(0, 2, everything, base(3), tile_rows)
+    hidden(2, 4, (0,), base(3), tile_rows)
+    pass_on(3)
+    hidden(2, 3, (1,), base(1), tile_rows, half - 1)
+    hidden(2, 3, (1,), base(0), rows)
+    pass_on(4)
+    for i in range(2, 4):
+        relay[i].wait_recv()
+    hidden(3, 4, (1,), base(1), tile_rows, half - 1)
+    hidden(3, 4, (1,), base(0), rows)
+    token_wait(half, 0)
+    pass_on(5)
+    norm(half)
+    hidden(0, 4, everything, base(half), rows)
+
+    passed = 2
+    for kind, c, k in sum_plan(chunks, half):
+        if kind == "down":
+            down(c)
+            if passed < chunks:
+                pass_on(4 + passed)
+                passed += 1
+        elif kind == "step":
+            sum_step(c, k)
+        elif kind == "end":
+            sum_end(c)
+        elif kind == "cross":
+            mix_cross()
+        else:
             mix_end()
-    for copy in sent:
+
+    ring_rows = half * rows - half_rows
+    part_count = count - 1
+    for ref, sem in (
+        (kv_all.at[0:part_count, 0:rows], kvf_send),
+        (kv_all.at[0:part_count, 0:rows], kvb_send),
+        (kv_all.at[:, 0 : 2 * rows], kvc_send),
+        (xn.at[0:ring_rows], fwd_send),
+        (xn.at[0:ring_rows], bwd_send),
+        (coefs.at[1:], coef_send),
+        (xn.at[0 : 3 * ff], core_send),
+        (xn.at[0 : 3 * ff], cross_send),
+        (xn.at[0 : 3 * ff], relay_send),
+        (y.at[:, 0:ring_rows], sum_r_send),
+        (y.at[:, 0:ring_rows], sum_l_send),
+    ):
+        remote(ref, ref, sem, sem, nxt).wait_send()
+    for copy in [kvr["x"], *q_copies, *mixes]:
         copy.wait_send()
-
-
-def turn_tables(group_rows):
-    half_width = ROPE // 2
-    frequency = rope_base ** (-jnp.arange(half_width, dtype=jnp.float32) / half_width)
-    positions = lax.axis_index("ep") * group_rows + jnp.arange(group_rows, dtype=jnp.int32)
-    angles = positions.astype(jnp.float32)[:, None] * jnp.tile(frequency, LANES // half_width)[None, :]
-    lane = jnp.arange(LANES, dtype=jnp.int32)[None, :]
-    inside = (lane >= NOPE) & (lane < NOPE + ROPE)
-    cosine = jnp.where(inside, jnp.cos(angles), jnp.where(lane < NOPE, 1.0, 0.0))
-    sine = jnp.where(inside, jnp.sin(angles), 0.0)
-    return cosine, jnp.where(lane < NOPE + half_width, -sine, sine)
-
-
-def coefficients(expert_ids, route_weights, expert_count):
-    experts = jnp.arange(expert_count, dtype=jnp.int32)
-    named = expert_ids.T[:, None, :] == experts[None, :, None]
-    return jnp.sum(jnp.where(named, route_weights.T[:, None, :], 0.0), axis=0)
+    with jax.named_scope("outs"):
+        for copy in outs:
+            copy.wait()
 
 
 def on_device_fused(
@@ -903,7 +1051,7 @@
     w_down_exp,
 ):
     count = lax.axis_size("ep")
-    chunks = 4
+    chunks = 8
     rows, depth = expert_input.shape
     ff = w_gate_exp.shape[2]
     heads = w_key.shape[1] // NOPE
@@ -915,8 +1063,9 @@
     pieces = 4 + chunks
     head_lanes = heads * LANES
     kv_width = rank + LANES
-    coef = coefficients(expert_ids, route_weights, count)
-    cosine, sine = turn_tables(group_rows)
+    half_width = ROPE // 2
+    frequency = np.float32(rope_base) ** (-np.arange(half_width, dtype=np.float32) / half_width)
+    frequency = jnp.asarray(np.tile(frequency, LANES // half_width)[None, :], jnp.float32)
     bf16, f32 = jnp.bfloat16, jnp.float32
     dma = pltpu.SemaphoreType.DMA
     vmem = pl.BlockSpec(memory_space=pltpu.VMEM)
@@ -924,18 +1073,31 @@
     return pl.pallas_call(
         functools.partial(layer_kernel, count, chunks),
         out_shape=[jax.ShapeDtypeStruct((rows, depth), bf16)] * 2,
-        in_specs=[vmem] * 15 + [hbm] * 3,
-        out_specs=[vmem, vmem],
+        in_specs=[vmem] * 5 + [hbm] * 5 + [vmem, hbm, vmem, vmem, vmem] + [hbm] * 3,
+        out_specs=[hbm, hbm],
         scratch_shapes=[
+            pltpu.VMEM((rows, depth), bf16),
+            pltpu.VMEM(w_query.shape, bf16),
+            pltpu.VMEM(w_query_rot.shape, bf16),
+            pltpu.VMEM(w_key.shape, bf16),
+            pltpu.VMEM(w_value.shape, bf16),
+            pltpu.VMEM(w_mix_out.shape, bf16),
+            pltpu.VMEM((rows, depth), bf16),
+            pltpu.VMEM((rows, depth), bf16),
+            pltpu.VMEM((group_rows, LANES), f32),
+            pltpu.VMEM((group_rows, LANES), f32),
+            pltpu.VMEM((count, rows), f32),
             pltpu.VMEM((group_rows, q_rank), bf16),
             pltpu.VMEM((q_rank, 2 * head_lanes), bf16),
             pltpu.VMEM((group_rows, head_lanes), bf16),
             pltpu.VMEM((count, group_rows, kv_width), bf16),
-            pltpu.VMEM((kv_width, 2 * head_lanes), bf16),
-            pltpu.VMEM((group_rows, 2 * head_lanes), bf16),
-            pltpu.VMEM((heads, group_rows, LANES), f32),
-            pltpu.VMEM((heads, group_rows, LANES), f32),
-            pltpu.VMEM((group_rows, heads * VD), bf16),
+            pltpu.VMEM((kv_width, head_lanes), bf16),
+            pltpu.VMEM((heads * VR, kv_width), bf16),
+            pltpu.VMEM((group_rows, head_lanes), bf16),
+            pltpu.VMEM((heads, VR, group_rows), bf16),
+            pltpu.VMEM((heads, 1, group_rows), f32),
+            pltpu.VMEM((heads, VR, group_rows), f32),
+            pltpu.VMEM((heads * VD, group_rows), bf16),
             pltpu.VMEM((4, rows, depth), bf16),
             pltpu.VMEM((2, rows, depth), bf16),
             pltpu.VMEM((rows, depth), bf16),
@@ -952,30 +1114,32 @@
             dma((3,)),
             dma((3,)),
             dma((2,)),
-            dma((half + 1, 2)),
-            dma((half + 1, 2)),
-            dma((half + 1, 2)),
-            dma((half + 1, 2)),
-            dma((count, 2)),
+            dma,
+            dma((half, 2)),
+            dma,
+            dma((half, 2)),
+            dma,
             dma((count, 2)),
             dma((3,)),
             dma((3,)),
+            dma((6,)),
+            dma((chunks + 1,)),
             dma((pieces,)),
-            dma((count,)),
-            dma((count,)),
-            dma((half + 1, 2)),
-            dma((half + 1, 2)),
-            dma((half + 1, 2)),
-            dma((half + 1, 2)),
+            dma,
+            dma,
+            dma,
+            dma((half, 2)),
+            dma,
+            dma((half, 2)),
+            dma,
             dma((pieces,)),
+            dma,
             dma((pieces,)),
+            dma,
             dma((pieces,)),
-            dma((pieces,)),
-            dma((pieces,)),
-            dma((pieces,)),
+            dma,
             dma((chunks, half)),
-            dma((chunks, half)),
-            dma((chunks, half)),
+            dma,
             dma((chunks, half)),
         ],
         compiler_params=pltpu.CompilerParams(
@@ -990,7 +1154,7 @@
     )(
         q_latent,
         kv_latent,
-        rope_key,
+        rope_key.T,
         q_gain.reshape(1, -1),
         kv_gain.reshape(1, -1),
         w_query,
@@ -998,11 +1162,11 @@
         w_key,
         w_value,
         w_mix_out,
-        cosine,
-        sine,
+        frequency,
         expert_input,
         ffn_gain.reshape(1, -1),
-        coef,
+        expert_ids.T,
+        route_weights.T,
         w_gate_exp,
         w_up_exp,
         w_down_exp,
@@ -1011,7 +1175,7 @@
 
 def fits(mesh):
     ep, tp = mesh.shape["ep"], mesh.shape["tp"]
-    return tp == 4 and ep % 2 == 0 and 4 <= ep <= 8
+    return tp == 4 and ep == 2 * tp
 
 
 def solution(mesh):

time: 139 us -> 118 us (0.85)
  Pallas kernels: 131 us -> 114 us
  other arithmetic: 2.45 us -> 0 us
    pallas_call x1, Pallas kernels: 131 us -> 114 us  [on_device_fused(): pl.pallas_call(functools.partial(layer_kernel, count, chunks), out_shape=...]
    select_n x2 -> x0, other arithmetic: 1.83 us -> none  [the longest x1 1.82 us: turn_tables(): return (cosine, jnp.where(lane < NOPE + half_width, -sine, sine))]
    unnamed x11 -> x4, local copies, waits for them, and re-layouts: 4.03 us -> 2.74 us
where the time goes in v1:
time: 118 us
  Pallas kernels  114 us (97%)
  local copies, waits for them, and re-layouts  2.74 us (2%)
    pallas_call x1, Pallas kernels, on_device_fused(): pl.pallas_call(functools.partial(layer_kernel, count, chunks), out_shape=...  114 us
    unnamed x4, local copies, waits for them, and re-layouts  2.74 us

profile of v1, /device:TPU:0, one launch (start us, length us, event | category | flops | bytes accessed | tf_op | source)
XLA Modules:
  0.0 117.6 jit_solution(8146278660003424640)
XLA Ops:
  0.6 114.2 %layer.1 = (bf16[128,2048]{1,0:T(8,128)(2,1)}, bf16[128,2048]{1,0:T(8,128)(2,1)}) custom-call(bf16[128,512]{1,0:T(8,128)(2,1)} %q_ref.1, bf16[128,256]{1,0:T(8,128)(2,1)} %kv_ref.1, bf16[32,128]{1,0:T(8,128)(2,1)} %bitcast.6, f32[1,512]{1,0:T(1,128)} %bitcast.8, f32[1,256]{1,0:T(1,128)} %bitcast.11, bf16[512,256]{1,0:T(8,128)(2,1)} %w_query_ref.1, ...), custom_call_target="tpu_custom_call" | custom-call | flops 12884901888 | bytes 12582912 | tf_op jit(solution)/shard_map/layer/pallas_call | solution.py:1073
  114.9 0.0 copy-start
  114.9 1.9 %copy.22 = bf16[128,2048]{1,0:T(8,128)(2,1)} copy(bf16[128,2048]{1,0:T(8,128)(2,1)} %get-tuple-element.4) | data formatting | bytes 1048576
  116.8 0.0 copy-done
  116.8 0.8 copy.23
Async XLA Ops:
  114.9 2.0 %copy-start = (bf16[128,2048]{1,0:T(8,128)(2,1)S(1)}, bf16[128,2048]{1,0:T(8,128)(2,1)}, u32[]{:S(2)}) copy-start(bf16[128,2048]{1,0:T(8,128)(2,1)} %get-tuple-element.5) | copy-start | bytes 1572868

commit v2 on v1

--- a/solution.py
+++ b/solution.py
@@ -350,8 +350,7 @@
     gate_ref,
     up_ref,
     down_ref,
-    mix_out_ref,
-    out_ref,
+    both_out_ref,
     x_now,
     w_query_now,
     w_rot_now,
@@ -419,12 +418,13 @@
     sum_l_recv,
 ):
     bf16, f32 = jnp.bfloat16, jnp.float32
+    mix_out_ref, out_ref = both_out_ref.at[0], both_out_ref.at[1]
     rows = x_ref.shape[0]
     half_rows = rows // 2
     half = count // 2
     ff = gate_ref.shape[2]
     fh = ff // 2
-    width = out_ref.shape[1] // chunks
+    width = x_ref.shape[1] // chunks
     group_rows = 4 * rows
     heads = w_key_ref.shape[1] // NOPE
     rank = kv_ref.shape[1]
@@ -462,6 +462,30 @@
         inputs.append(pltpu.make_async_copy(src, dst, in_sem.at[i]))
         inputs[-1].start()
 
+    def go(copy):
+        copy.start()
+        return copy
+
+    def half_of(h):
+        return pl.ds(h * half_rows, half_rows)
+
+    def forward(step, h):
+        src = x_ref.at[half_of(h)] if step == 1 else raw.at[step - 1, half_of(h)]
+        return remote(
+            src, raw.at[step, half_of(h)], fwd_send, fwd_recv.at[step - 1, h], nxt
+        )
+
+    def backward(step, h):
+        src = x_ref.at[half_of(h)] if step == 1 else raw.at[count - step + 1, half_of(h)]
+        return remote(
+            src, raw.at[count - step, half_of(h)], bwd_send, bwd_recv.at[step - 1, h], prv
+        )
+
+    pl.semaphore_wait(barrier, count + 1)
+    ring = {}
+    ring["f", 1, 0] = go(forward(1, 0))
+    ring["b", 1, 1] = go(backward(1, 1))
+
     def rows_of(index):
         return pl.ds(pl.multiple_of(index * rows, rows), rows)
 
@@ -509,14 +533,6 @@
     for k in range(TOPK):
         coef += jnp.where(ids_ref[k : k + 1, :] == expert_id, route_ref[k : k + 1, :], 0.0)
     coef_ref[...] = coef
-    pl.semaphore_wait(barrier, count + 1)
-
-    def go(copy):
-        copy.start()
-        return copy
-
-    def half_of(h):
-        return pl.ds(h * half_rows, half_rows)
 
     part_rows = (own_rows, cross_rows)
 
@@ -547,21 +563,9 @@
             core_peer,
         )
 
-    def forward(step, h):
-        src = x_ref.at[half_of(h)] if step == 1 else raw.at[step - 1, half_of(h)]
-        return remote(
-            src, raw.at[step, half_of(h)], fwd_send, fwd_recv.at[step - 1, h], nxt
-        )
-
-    def backward(step, h):
-        src = x_ref.at[half_of(h)] if step == 1 else raw.at[count - step + 1, half_of(h)]
-        return remote(
-            src, raw.at[count - step, half_of(h)], bwd_send, bwd_recv.at[step - 1, h], prv
-        )
-
     def piece(i, slot):
         if i < 4:
-            return wgu.at[slot, i // 2, :, pl.ds((i % 2) * fh, fh)]
+            return wgu.at[slot, i // 2, i % 2]
         return wd.at[i - 4, pl.ds(slot * ff, ff)]
 
     def own_piece(i):
@@ -570,7 +574,7 @@
             return ref.at[0, :, pl.ds((i // 2) * fh, fh)]
         return down_ref.at[0, :, pl.ds((i - 4) * width, width)]
 
-    kvr, ring = {}, {}
+    kvr = {}
     kvr["x"] = go(
         remote(
             kv_all.at[0, own_rows],
@@ -587,8 +591,6 @@
         go(remote(q_all.at[own_rows], q_all.at[own_rows], q_send.at[i], q_recv.at[i], peer))
         for i, peer in enumerate((core_peer, cross_peer))
     ]
-    ring["f", 1, 0] = go(forward(1, 0))
-    ring["b", 1, 1] = go(backward(1, 1))
     to_coefs = [
         go(
             remote(
@@ -656,6 +658,8 @@
     kvr["f", 1, 1] = go(kv_forward(1, 1))
     kvr["b", 1, 1] = go(kv_backward(1, 1))
     kvr["c", 0, 1] = go(kv_core(0, 1))
+    ring["f", 1, 1] = go(forward(1, 1))
+    ring["b", 1, 0] = go(backward(1, 0))
 
     cos_ref[...], sin_ref[...] = turn_table(0, group_rows)
     wq_cat[...] = jnp.zeros_like(wq_cat)
@@ -781,7 +785,8 @@
             def _(tile):
                 part = pl.ds(pl.multiple_of(first + tile * size, rows), size)
                 for h in halves:
-                    both = jnp.dot(xn[part, :], wgu[slot, h], preferred_element_type=f32)
+                    weight = jnp.concatenate([wgu[slot, h, 0], wgu[slot, h, 1]], axis=1)
+                    both = jnp.dot(xn[part, :], weight, preferred_element_type=f32)
                     gate = both[:, :fh]
                     at = pl.ds(pl.multiple_of((slot * 2 + h) * fh, fh), fh)
                     hid[part, at] = (gate * jax.nn.sigmoid(gate) * both[:, fh:]).astype(bf16)
@@ -844,22 +849,26 @@
         outs.append(pltpu.make_async_copy(mix_stage, mix_out_ref, out_sem.at[chunks]))
         outs[-1].start()
 
-    def down(c):
+    def down_tile(c, pair):
+        part = pl.ds(pl.multiple_of(pair * tile_rows, tile_rows), tile_rows)
+        acc = jnp.dot(hid[part, :], wd[c], preferred_element_type=f32)
+        y[c, part, :] = (acc * coef_col[part, :]).astype(bf16)
+
+    def down_head(c):
         local[4 + c].wait()
         to_core[4 + c].wait_recv()
         relay[4 + c].wait_recv()
-
-        def tile(pair):
-            part = pl.ds(pl.multiple_of(pair * tile_rows, tile_rows), tile_rows)
-            acc = jnp.dot(hid[part, :], wd[c], preferred_element_type=f32)
-            y[c, part, :] = (acc * coef_col[part, :]).astype(bf16)
-
-        tile(0)
+        down_tile(c, 0)
         sum_start(c)
 
+    def down_rest(c):
         @pl.loop(1, half)
         def _(back):
-            tile(half - back)
+            down_tile(c, half - back)
+
+    def down(c):
+        down_head(c)
+        down_rest(c)
 
     def block(slot, h=None):
         if h is None:
@@ -932,33 +941,32 @@
     for i in range(4):
         local[i].wait()
         to_core[i].wait_recv()
+    hidden(0, 2, everything, base(0), rows)
     kv_step(1, 0)
-    ring["f", 1, 1] = go(forward(1, 1))
-    ring["b", 1, 0] = go(backward(1, 0))
-    hidden(0, 2, everything, base(0), rows)
     make_queries_here()
+    kv_step(1, 1)
+    token_step(1, 0)
     attend_slot(0)
-    kv_step(1, 1)
     attend_slot(1)
-    kv_step(2, 0)
-    token_step(1, 0)
-    attend_slot(count - 1)
     remote(coefs.at[1:], coefs.at[1:], coef_send, coef_recv, nxt).wait_recv()
     for slot in range(1, count):
         coefficient(slot)
-
+    attend_slot(count - 1)
+
+    kv_step(2, 0)
+    pass_on(0)
     token_wait(1, 1)
     pair_norm(1)
-    pass_on(0)
-    hidden(0, 2, everything, base(1), tile_rows)
     kv_step(2, 1)
     token_pass(1, 1)
+    hidden(0, 2, everything, base(1), tile_rows)
     attend_slot(2)
+    attend_slot(count - 2)
+    token_wait(2, 0)
     kv_step(3, 0)
-    attend_slot(count - 2)
-    token_step(2, 0)
     pass_on(1)
     kv_step(3, 1)
+    token_pass(2, 0)
     for i in range(2):
         relay[i].wait_recv()
     hidden(2, 4, (0,), base(0), rows)
@@ -966,36 +974,40 @@
     attend_slot(3)
     attend_slot(count - 3)
     token_step(2, 1)
+    kv_step(4, 0)
+    kv_step(4, 1)
     pair_norm(2)
     hidden(0, 2, everything, base(2), tile_rows)
-    kv_step(4, 0)
-    kv_step(4, 1)
     pass_on(2)
     hidden(2, 4, (0,), base(2), tile_rows)
+    attend_slot(4)
     token_step(3, 0)
-    attend_slot(4)
     mix_start()
-    token_step(3, 1)
+    token_wait(3, 1)
     pair_norm(3)
     hidden(0, 2, everything, base(3), tile_rows)
+    pass_on(3)
     hidden(2, 4, (0,), base(3), tile_rows)
-    pass_on(3)
     hidden(2, 3, (1,), base(1), tile_rows, half - 1)
     hidden(2, 3, (1,), base(0), rows)
     pass_on(4)
+    token_wait(half, 0)
+    norm(half)
+    hidden(0, 3, everything, base(half), rows)
     for i in range(2, 4):
         relay[i].wait_recv()
+    hidden(3, 4, everything, base(half), rows)
+    hidden(3, 4, (1,), base(0), rows)
+    down_head(0)
+    pass_on(5)
     hidden(3, 4, (1,), base(1), tile_rows, half - 1)
-    hidden(3, 4, (1,), base(0), rows)
-    token_wait(half, 0)
-    pass_on(5)
-    norm(half)
-    hidden(0, 4, everything, base(half), rows)
+    down_rest(0)
 
     passed = 2
     for kind, c, k in sum_plan(chunks, half):
         if kind == "down":
-            down(c)
+            if c > 0:
+                down(c)
             if passed < chunks:
                 pass_on(4 + passed)
                 passed += 1
@@ -1070,11 +1082,11 @@
     dma = pltpu.SemaphoreType.DMA
     vmem = pl.BlockSpec(memory_space=pltpu.VMEM)
     hbm = pl.BlockSpec(memory_space=pl.ANY)
-    return pl.pallas_call(
+    both = pl.pallas_call(
         functools.partial(layer_kernel, count, chunks),
-        out_shape=[jax.ShapeDtypeStruct((rows, depth), bf16)] * 2,
+        out_shape=jax.ShapeDtypeStruct((2, rows, depth), bf16),
         in_specs=[vmem] * 5 + [hbm] * 5 + [vmem, hbm, vmem, vmem, vmem] + [hbm] * 3,
-        out_specs=[hbm, hbm],
+        out_specs=hbm,
         scratch_shapes=[
             pltpu.VMEM((rows, depth), bf16),
             pltpu.VMEM(w_query.shape, bf16),
@@ -1103,7 +1115,7 @@
             pltpu.VMEM((rows, depth), bf16),
             pltpu.VMEM((count, rows, depth), bf16),
             pltpu.VMEM((count * rows, depth), bf16),
-            pltpu.VMEM((4, 2, depth, ff), bf16),
+            pltpu.VMEM((4, 2, 2, depth, ff // 2), bf16),
             pltpu.VMEM((chunks, 4 * ff, width), bf16),
             pltpu.VMEM((count * rows, 4 * ff), bf16),
             pltpu.VMEM((chunks, count * rows, width), bf16),
@@ -1171,6 +1183,7 @@
         w_up_exp,
         w_down_exp,
     )
+    return both[0], both[1]
 
 
 def fits(mesh):

time: 118 us -> 117 us (level)
    unnamed x4 -> x0, local copies, waits for them, and re-layouts: 2.74 us -> none
    squeeze x0 -> x1, local copies, waits for them, and re-layouts: none -> 2.28 us  [on_device_fused(): return (both[0], both[1])]
where the time goes in v2:
time: 117 us
  Pallas kernels  114 us (97%)
  local copies, waits for them, and re-layouts  2.28 us (2%)
    pallas_call x1, Pallas kernels, on_device_fused(): pl.pallas_call(functools.partial(layer_kernel, count, chunks), out_shape=...  114 us

profile of v2, /device:TPU:0, one launch (start us, length us, event | category | flops | bytes accessed | tf_op | source)
XLA Modules:
  0.0 117.2 jit_solution(10028802838632220876)
XLA Ops:
  0.6 114.3 %layer.1 = bf16[2,128,2048]{2,1,0:T(8,128)(2,1)} custom-call(bf16[128,512]{1,0:T(8,128)(2,1)} %q_ref.1, bf16[128,256]{1,0:T(8,128)(2,1)} %kv_ref.1, bf16[32,128]{1,0:T(8,128)(2,1)} %bitcast.10, f32[1,512]{1,0:T(1,128)} %bitcast.12, f32[1,256]{1,0:T(1,128)} %bitcast.15, bf16[512,256]{1,0:T(8,128)(2,1)} %w_query_ref.1, bf16[512,128]{1,0:T(8,128)(2,1)} %w_rot_ref.1, ...), custom_call_target="tpu_custom_call" | custom-call | flops 12884901888 | bytes 12582912 | tf_op jit(solution)/shard_map/layer/pallas_call | solution.py:1085
  114.9 2.3 %slice_bitcast_fusion = (bf16[128,2048]{1,0:T(8,128)(2,1)}, bf16[128,2048]{1,0:T(8,128)(2,1)}) fusion(bf16[2,128,2048]{2,1,0:T(8,128)(2,1)} %layer.1), kind=kLoop, calls=%fused_computation | loop fusion | bytes 2097152 | tf_op jit(solution)/shard_map/squeeze | solution.py:1186
